TPU v7x, 32 devices: a whole 2x2x4 slice. The times are simulated.
32 devices in a mesh: sp: 8 (over z, x), tp: 4 (over y, core).
Axes of the slice: x: 2, y: 2, z: 4, core: 2. Of those that a mesh axis runs over, the one named last changes fastest.
Arguments:
- prompt: bfloat16 [4, 4096, 4096], P(None, 'sp'), may hold values from -6 to 6
- key_weight: bfloat16 [4096, 1024], P(None, 'tp'), may hold values from -0.09375 to 0.09375
- value_weight: bfloat16 [4096, 2048], P(None, 'tp'), may hold values from -0.09375 to 0.09375
- input_gate_weight: bfloat16 [4096, 16], P(None, 'tp'), may hold values from -0.09375 to 0.09375
- forget_gate_weight: bfloat16 [4096, 16], P(None, 'tp'), may hold values from -0.09375 to 0.09375
- forget_bias: float32 [16], P('tp'), may hold values from 3 to 11
- key_taps: bfloat16 [3, 1024], P(None, 'tp'), may hold values from -3 to 3
- extra_decay: float32 [4, 4096, 16], P(None, 'sp', 'tp'), may hold values from -1.5 to 0
- new_query: bfloat16 [4, 16, 64], P(None, 'tp'), may hold values from -6 to 6
- new_key: bfloat16 [4, 16, 64], P(None, 'tp'), may hold values from -6 to 6
- new_value: bfloat16 [4, 16, 128], P(None, 'tp', 'sp'), may hold values from -6 to 6
- new_input_gate: float32 [4, 16], P(None, 'tp'), may hold values from 2 to 7
- new_forget_gate: float32 [4, 16], P(None, 'tp'), may hold values from -2 to 4
- out_weight: bfloat16 [16, 128, 4096], P('tp', 'sp'), may hold values from -0.125 to 0.125
Outputs:
- cache_memory: bfloat16 [4, 16, 64, 128], P(None, 'tp', None, 'sp')
- cache_norm: bfloat16 [4, 16, 64], P(None, 'tp', 'sp')
- cache_peak: float32 [4, 16], P(None, 'tp')
- read_out: bfloat16 [4, 4096], P(None, ('sp', 'tp'))
All inputs are finite; a program needn't handle non-finite values.
Results may differ from a plain program's by a relative error of at most 0.012.
The roundings to bfloat16 on the way count: a program that leaves them out, or rounds other values in their place, can miss the bound.
Values may be sent and summed in bfloat16 or wider, within the bound.
A program may use at most 64 MiB of HBM per device.

v0:
```python
import jax
import jax.numpy as jnp
from jax import lax
from jax.sharding import PartitionSpec as P

KEY_DIM = 64


def with_halo(shard, sides, width):
    for axis, dim in sides:
        devices, length = (lax.axis_size(axis), shard.shape[dim])
        up = [(i, (i + 1) % devices) for i in range(devices - 1)]
        down = [(j, i) for i, j in up]
        last = lax.slice_in_dim(shard, length - width, length, axis=dim)
        leading = lax.slice_in_dim(shard, 0, width, axis=dim)
        before = lax.ppermute(last, axis, up)
        after = lax.ppermute(leading, axis, down)
        shard = jnp.concatenate([before, shard, after], axis=dim)
    return shard


def carried_in(shard, axis, combine, identity):
    devices, here = (lax.axis_size(axis), lax.axis_index(axis))
    everything = lax.all_gather(shard, axis)
    start = jnp.broadcast_to(jnp.asarray(identity, shard.dtype), shard.shape)

    def hop(k, before):
        at = devices - 1 - k
        reached = at > here
        new = combine(before, everything[at])
        return jnp.where(reached, new, before)

    return lax.fori_loop(0, devices, hop, start)


def widen(rounded):
    return lax.optimization_barrier(rounded).astype(jnp.float32)


def project(seq_rows, key_weight, value_weight, input_gate_weight, forget_gate_weight):
    seq_count, pos_count, width = seq_rows.shape
    flat_rows = seq_rows.reshape(seq_count * pos_count, width)
    key_raw = jnp.dot(flat_rows, key_weight, preferred_element_type=jnp.float32).astype(
        jnp.bfloat16
    )
    values = jnp.dot(flat_rows, value_weight, preferred_element_type=jnp.float32).astype(
        jnp.bfloat16
    )
    gate_weight = jnp.concatenate([input_gate_weight, forget_gate_weight], axis=1)
    gate_pre = jnp.dot(flat_rows, gate_weight, preferred_element_type=jnp.float32).astype(
        jnp.bfloat16
    )
    return (
        key_raw.reshape(seq_count, pos_count, -1),
        values.reshape(seq_count, pos_count, -1),
        gate_pre.reshape(seq_count, pos_count, -1),
    )


def key_conv(padded, key_taps):
    tap_f32 = key_taps.astype(jnp.float32)
    mixed = tap_f32[0] * padded[:, :-2] + tap_f32[1] * padded[:, 1:-1] + tap_f32[2] * padded[:, 2:]
    return (jax.nn.silu(mixed) * KEY_DIM ** (-0.5)).astype(jnp.bfloat16)


def gate_parts(gate_pre, forget_bias, extra):
    head_count = extra.shape[-1]
    gate_f32 = widen(gate_pre)
    input_pre = gate_f32[..., :head_count]
    log_forget = jax.nn.log_sigmoid(gate_f32[..., head_count:] + forget_bias) + extra
    return (input_pre, log_forget)


def suffix_of(log_forget):
    return jnp.sum(log_forget, axis=1, keepdims=True) - jnp.cumsum(log_forget, axis=1)


def add_later(earlier, latter):
    return earlier + latter


def body(
    prompt,
    key_weight,
    value_weight,
    input_gate_weight,
    forget_gate_weight,
    forget_bias,
    key_taps,
    extra_decay,
    new_query,
    new_key,
    new_value,
    new_input_gate,
    new_forget_gate,
    out_weight,
):
    seq_count = prompt.shape[0]
    head_count = extra_decay.shape[-1]
    key_size = new_key.shape[2]
    sp_count = lax.axis_size("sp")
    sp_index = lax.axis_index("sp")
    key_cols = key_size // sp_count
    key_raw, values, gate_pre = project(
        prompt, key_weight, value_weight, input_gate_weight, forget_gate_weight
    )
    input_pre, log_forget = gate_parts(gate_pre, forget_bias, extra_decay)
    padded = with_halo(key_raw, (("sp", 1),), 1)
    key_rows = key_conv(padded, key_taps)
    seg_total = jnp.sum(log_forget, axis=1)
    later_sum = carried_in(seg_total, "sp", add_later, jnp.zeros_like(seg_total))
    gate_log = input_pre + suffix_of(log_forget) + later_sum[:, None, :]
    peak_log = lax.pmax(jnp.max(gate_log, axis=1), "sp")
    scale = jnp.exp(gate_log - peak_log[:, None, :])
    pos_count = scale.shape[1]
    key_quartet = key_rows.reshape(seq_count, pos_count, head_count, key_size)
    value_four = values.reshape(seq_count, pos_count, head_count, -1)
    weighted_rows = (value_four * scale[..., None]).astype(jnp.bfloat16)
    memory_part = jnp.einsum(
        "slhk,slhv->shkv", key_quartet, weighted_rows, preferred_element_type=jnp.float32
    )
    normer_part = jnp.einsum(
        "slh,slhk->shk", scale, key_quartet.astype(jnp.float32), precision=lax.Precision.HIGHEST
    )
    memory_matrix, normer = (
        lax.psum_scatter(memory_part, "sp", scatter_dimension=3, tiled=True),
        lax.psum_scatter(normer_part, "sp", scatter_dimension=2, tiled=True),
    )
    forget_new = jax.nn.log_sigmoid(new_forget_gate)
    new_peak = jnp.maximum(forget_new + peak_log, new_input_gate)
    old_scale = jnp.exp(forget_new + peak_log - new_peak)
    new_scale = jnp.exp(new_input_gate - new_peak)
    key_new = new_key.astype(jnp.float32)
    key_new_slice = lax.dynamic_slice_in_dim(key_new, sp_index * key_cols, key_cols, 2)
    value_new = new_value.astype(jnp.float32)
    memory_next = (
        old_scale[:, :, None, None] * memory_matrix
        + new_scale[:, :, None, None] * key_new[:, :, :, None] * value_new[:, :, None, :]
    )
    normer_next = old_scale[:, :, None] * normer + new_scale[:, :, None] * key_new_slice
    query = new_query.astype(jnp.float32)
    query_slice = lax.dynamic_slice_in_dim(query, sp_index * key_cols, key_cols, 2)
    numer = jnp.sum(query[:, :, :, None] * memory_next, axis=2)
    denom = lax.psum(jnp.sum(query_slice * normer_next, axis=-1), "sp")
    read = (numer / jnp.maximum(jnp.abs(denom), 1.0)[:, :, None]).astype(jnp.bfloat16)
    partial_value = jnp.einsum("shv,hvd->sd", read, out_weight, preferred_element_type=jnp.float32)
    read_out = lax.psum_scatter(
        partial_value, ("sp", "tp"), scatter_dimension=1, tiled=True
    ).astype(jnp.bfloat16)
    return (memory_matrix.astype(jnp.bfloat16), normer.astype(jnp.bfloat16), peak_log, read_out)


def solution(mesh):
    placed = (
        P(None, "sp", None),
        P(None, "tp"),
        P(None, "tp"),
        P(None, "tp"),
        P(None, "tp"),
        P("tp"),
        P(None, "tp"),
        P(None, "sp", "tp"),
        P(None, "tp", None),
        P(None, "tp", None),
        P(None, "tp", "sp"),
        P(None, "tp"),
        P(None, "tp"),
        P("tp", "sp", None),
    )
    return jax.shard_map(
        body,
        mesh=mesh,
        in_specs=placed,
        out_specs=(
            P(None, "tp", None, "sp"),
            P(None, "tp", "sp"),
            P(None, "tp"),
            P(None, ("sp", "tp")),
        ),
        check_vma=False,
    )
```

profile of v0, /device:TPU:0, one launch (start us, length us, event | category | flops | bytes accessed | tf_op | source)
XLA Modules:
  0.0 337.2 jit_solution(1434747323576599410)
XLA Ops:
  7.2 0.0 copy-start
  7.2 0.0 reduce-scatter.6.cloned.1.call-start
  7.2 1.5 copy-done
  8.8 8.2 %convolution_convert_fusion.1 = bf16[2048,256]{1,0:T(8,128)(2,1)S(1)} fusion(bf16[2048,4096]{1,0:T(8,128)(2,1)} %bitcast.42, bf16[4096,256]{1,0:T(8,128)(2,1)S(1)} %copy-done), kind=kOutput, calls=%fused_computation.5 | convolution fusion | flops 4295491584 | bytes 19922944 | tf_op jit(solution)/shard_map/dot_general | solution.py:43
  17.0 0.0 copy-start.2
  17.0 1.1 copy-done.2
  18.1 1.3 collective-permute-start.1
  19.4 5.5 %collective-permute-start = (bf16[4,1,256]{2,1,0:T(2,128)(2,1)S(1)}, bf16[4,1,256]{2,1,0:T(2,128)(2,1)S(1)}, u32[]{:S(2)}, u32[]{:S(2)}) collective-permute-start(bf16[4,1,256]{2,1,0:T(2,128)(2,1)S(1)} %get-tuple-element.140), channel_id=1, source_target_pairs={{0,4},{4,8},{8,12},{12,16},{16,20},{20,24},{24,28},{1,5},{5,9},{9,... | collective-permute-start | bytes 6152 | tf_op jit(solution)/shard_map/ppermute | solution.py:16
  24.9 0.0 copy-start.5
  25.0 0.0 copy-start.13
  25.0 10.2 %convolution_convert_fusion.2 = bf16[8,2048]{1,0:T(8,128)(2,1)S(1)} fusion(bf16[2048,4096]{1,0:T(8,128)(2,1)} %bitcast.43, bf16[4096,4]{0,1:T(4,128)(2,1)S(1)} %copy-done.3, bf16[4096,4]{0,1:T(4,128)(2,1)S(1)} %copy-done.4), kind=kOutput, calls=%fused_computation.6 | convolution fusion | flops 134365184 | bytes 16875520 | tf_op jit(solution)/shard_map/dot_general | solution.py:50
  35.2 0.2 fusion.19
  35.4 27.0 %all-gather.1 = f32[8,4,4]{2,1,0:T(4,128)S(1)} all-gather(f32[1,4,4]{2,1,0:T(4,128)S(1)} %bitcast.53), channel_id=2, replica_groups=mesh['sp'=8,'tp'=4] {'sp'}, dimensions={0}, use_global_device_ids=true | all-gather | bytes 576 | tf_op jit(solution)/shard_map/all_gather | solution.py:24
  62.4 0.3 while.16
  62.7 4.8 %reduce-window.6 = f32[4,4,4,128]{3,2,1,0:T(4,128)S(1)} reduce-window(f32[4,4,4,128]{3,2,1,0:T(4,128)S(1)} %reshape.55, f32[]{:T(128)} %constant.67.clone.1), window={size=1x1x1x128 pad=0_0x0_0x0_0x127_0}, to_apply=%region_1.2 | reduce-window | flops 1040384 | bytes 65540 | tf_op jit(solution)/shard_map/reduce-window
  67.6 0.2 slice_reduce_fusion
  67.8 0.7 reduce-window.9
  68.5 0.1 broadcast_add_fusion
  68.6 0.2 fusion.18
  68.7 14.8 %fusion = f32[2048,512]{1,0:T(8,128)} fusion(bf16[2048,4096]{1,0:T(8,128)(2,1)} %bitcast.44, bf16[4096,512]{1,0:T(8,128)(2,1)} %param.18), kind=kOutput, calls=%fused_computation.4 | convolution fusion | flops 8592031744 | bytes 25165824 | tf_op jit(solution)/shard_map/dot_general | solution.py:46
  83.6 19.5 %pmax.7 = f32[4,4]{1,0:T(4,128)S(1)} all-reduce(f32[4,4]{1,0:T(4,128)S(1)} %fusion.18), channel_id=1, replica_groups=mesh['sp'=8,'tp'=4] {'sp'}, use_global_device_ids=true, to_apply=%region_6.7 | all-reduce | flops 16 | bytes 128 | tf_op jit(solution)/shard_map/pmax | solution.py:113
  103.1 0.1 subtract_exponential_fusion
  103.2 5.2 %reshape.57 = f32[4,512,4,128]{3,2,1,0:T(4,128)} reshape(f32[2048,512]{1,0:T(8,128)} %fusion) | data formatting | bytes 8388608 | tf_op jit(solution)/shard_map/convert_element_type | solution.py:118
  108.5 5.2 %copy.23 = f32[4,512,4,128]{1,3,2,0:T(8,128)} copy(f32[4,512,4,128]{3,2,1,0:T(4,128)} %reshape.57) | data formatting | bytes 8388608 | tf_op jit(solution)/shard_map/convert_element_type | solution.py:118
  113.7 0.0 collective-permute-done.1
  113.7 0.0 collective-permute-done
  113.7 3.7 %multiply_convert_fusion.2 = bf16[4,512,256]{2,1,0:T(8,128)(2,1)S(1)} fusion(bf16[4,512,256]{2,1,0:T(8,128)(2,1)} %bitcast.48, bf16[4,1,256]{2,1,0:T(2,128)(2,1)S(1)} %collective-permute-done.1, bf16[4,1,256]{2,1,0:T(2,128)(2,1)S(1)} %collective-permute-done, f32[256]{0:T(256)S(1)} %bitcast.58, f32[256]{0:T(256)S(1)} %bitcast.57, f32[256]{0:T(256)S(1)} %bitcast.56), kind=kLoop, calls=%fused_computation.9 | loop fusion | flops 10485760 | bytes 2104320 | tf_op jit(solution)/shard_map/convert_element_type | solution.py:63
  117.4 1.3 copy.22
  118.8 0.0 copy-start.12
  118.8 4.3 %fusion.1 = f32[4,4,64,128]{2,3,1,0:T(8,128)} fusion(bf16[4,512,4,64]{1,3,2,0:T(8,128)(2,1)} %bitcast.45, f32[4,512,4,128]{1,3,2,0:T(8,128)} %copy.23, f32[4,512,4]{1,2,0:T(4,128)S(1)} %subtract_exponential_fusion), kind=kOutput, calls=%fused_computation.7 | convolution fusion | flops 136314880 | bytes 5799936 | tf_op jit(solution)/shard_map/slhk,slhv->shkv/dot_general | solution.py:119
  123.1 0.0 reduce-scatter.6.cloned.1.call-update
  123.1 0.0 reduce-scatter.8.cloned.1.call-start
  123.3 0.6 dynamic-slice
  124.5 0.1 broadcast_multiply_fusion
  124.6 0.0 copy-done.1
  124.6 0.9 fusion.10
  125.5 17.6 %all-reduce = f32[4,4,64]{2,1,0:T(4,128)S(1)} all-reduce(f32[4,4,64]{2,1,0:T(4,128)S(1)} %bitcast.55), channel_id=4, replica_groups=mesh['sp'=8,'tp'=4] {'sp'}, use_global_device_ids=true, to_apply=%region_8.9.clone | all-reduce | flops 1024 | bytes 8192
  143.2 0.2 multiply_reduce_fusion.1
  143.4 0.0 copy-done.10
  143.4 19.2 %psum.7 = f32[4,4]{1,0:T(4,128)S(1)} all-reduce(f32[4,4]{1,0:T(4,128)S(1)} %multiply_reduce_fusion.1), channel_id=1, replica_groups=mesh['sp'=8,'tp'=4] {'sp'}, use_global_device_ids=true, to_apply=%region_11.12 | all-reduce | flops 16 | bytes 128 | tf_op jit(solution)/shard_map/psum | solution.py:144
  162.6 22.6 %reduce-scatter.6.cloned.1.call-done = f32[4,4,64,16]{2,3,1,0:T(8,128)} async-done(((f32[4,4,64,128]{2,3,1,0:T(8,128)}), f32[4,4,64,16]{2,3,1,0:T(8,128)}) %reduce-scatter.6.cloned.1.call-update) | async-done | bytes 65552 | tf_op jit(solution)/shard_map/reduce_scatter | solution.py:126
  185.2 1.8 multiply_reduce_fusion
  187.0 0.1 divide_convert_fusion
  187.0 4.1 %convolution_bitcast_fusion = f32[4096,4]{1,0:T(8,128)} fusion(bf16[4,16,4096]{2,1,0:T(8,128)(2,1)} %param.29, bf16[4,4,16]{2,1,0:T(4,128)(2,1)S(1)} %divide_convert_fusion), kind=kOutput, calls=%fused_computation.1 | convolution fusion | flops 2097152 | bytes 590336 | tf_op jit(solution)/shard_map/shv,hvd->sd/dot_general | solution.py:146
  191.1 0.0 reduce-scatter.8.cloned.1.call-update
  191.2 0.7 dynamic-slice_convert_fusion
  191.8 137.0 %reduce-scatter.8.cloned.1.call-done = f32[128,4]{1,0:T(8,128)} async-done(((f32[4096,4]{1,0:T(8,128)}), f32[128,4]{1,0:T(8,128)}) %reduce-scatter.8.cloned.1.call-update) | async-done | bytes 2064
  328.9 1.5 copy.30
  (40 shorter events, 0.3 us)
Async XLA Ops:
  7.2 1.6 copy-start
  7.2 178.0 %reduce-scatter.6.cloned.1.call-start = ((), (), s32[]{:S(2)}) async-start(), calls=%async_computation.2 | async-start | bytes 1179648 | tf_op jit(solution)/shard_map/reduce_scatter | solution.py:126
  8.8 16.2 %copy-start.3 = (bf16[4096,4]{0,1:T(4,128)(2,1)S(1)}, bf16[4096,4]{0,1:T(4,128)(2,1)}, u32[]{:S(2)}) copy-start(bf16[4096,4]{0,1:T(4,128)(2,1)} %param.20) | copy-start | bytes 98308
  8.8 16.2 %copy-start.4 = (bf16[4096,4]{0,1:T(4,128)(2,1)S(1)}, bf16[4096,4]{0,1:T(4,128)(2,1)}, u32[]{:S(2)}) copy-start(bf16[4096,4]{0,1:T(4,128)(2,1)} %param.19) | copy-start | bytes 98308
  17.0 1.1 copy-start.2
  18.1 95.6 %collective-permute-start.1 = (bf16[4,1,256]{2,1,0:T(2,128)(2,1)S(1)}, bf16[4,1,256]{2,1,0:T(2,128)(2,1)S(1)}, u32[]{:S(2)}, u32[]{:S(2)}) collective-permute-start(bf16[4,1,256]{2,1,0:T(2,128)(2,1)S(1)} %get-tuple-element.141), channel_id=1, source_target_pairs={{4,0},{8,4},{12,8},{16,12},{20,16},{24,20},{28,24},{5,1},{9,5},{13... | collective-permute-start | bytes 6152 | tf_op jit(solution)/shard_map/ppermute | solution.py:17
  19.4 94.3 %collective-permute-start = (bf16[4,1,256]{2,1,0:T(2,128)(2,1)S(1)}, bf16[4,1,256]{2,1,0:T(2,128)(2,1)S(1)}, u32[]{:S(2)}, u32[]{:S(2)}) collective-permute-start(bf16[4,1,256]{2,1,0:T(2,128)(2,1)S(1)} %get-tuple-element.140), channel_id=1, source_target_pairs={{0,4},{4,8},{8,12},{12,16},{16,20},{20,24},{24,28},{1,5},{5,9},{9,... | collective-permute-start | bytes 6152 | tf_op jit(solution)/shard_map/ppermute | solution.py:16
  24.9 10.2 %copy-start.5 = (f32[4,512,4]{1,2,0:T(4,128)S(1)}, f32[4,512,4]{1,2,0:T(4,128)}, u32[]{:S(2)}) copy-start(f32[4,512,4]{1,2,0:T(4,128)} %param.23) | copy-start | bytes 98308
  25.0 10.2 %copy-start.13 = (f32[4]{0:T(128)S(1)}, f32[4]{0:T(128)}, u32[]{:S(2)}) copy-start(f32[4]{0:T(128)} %param.21) | copy-start | bytes 52
  68.7 34.5 %copy-start.8 = (bf16[3,256]{1,0:T(4,128)(2,1)S(1)}, bf16[3,256]{1,0:T(4,128)(2,1)}, u32[]{:S(2)}) copy-start(bf16[3,256]{1,0:T(4,128)(2,1)} %param.22) | copy-start | bytes 4612
  103.1 21.4 %copy-start.6 = (f32[4,4]{1,0:T(4,128)}, f32[4,4]{1,0:T(4,128)S(1)}, u32[]{:S(2)}) copy-start(f32[4,4]{1,0:T(4,128)S(1)} %pmax.7) | copy-start | bytes 196
  118.8 4.4 %copy-start.9 = (bf16[4,4,64]{2,1,0:T(4,128)(2,1)S(1)}, bf16[4,4,64]{2,1,0:T(4,128)(2,1)}, u32[]{:S(2)}) copy-start(bf16[4,4,64]{2,1,0:T(4,128)(2,1)} %param.24) | copy-start | bytes 6148
  118.8 4.4 %copy-start.7 = (bf16[4,4,64]{2,1,0:T(4,128)(2,1)S(1)}, bf16[4,4,64]{2,1,0:T(4,128)(2,1)}, u32[]{:S(2)}) copy-start(bf16[4,4,64]{2,1,0:T(4,128)(2,1)} %param.25) | copy-start | bytes 6148
  118.8 4.5 %copy-start.14 = (u32[32]{0:T(128)S(1)}, u32[32]{0:T(128)}, u32[]{:S(2)}) copy-start(u32[32]{0:T(128)} %constant.76) | copy-start | bytes 388
  118.8 5.7 %copy-start.11 = (f32[4,4]{1,0:T(4,128)S(1)}, f32[4,4]{1,0:T(4,128)}, u32[]{:S(2)}) copy-start(f32[4,4]{1,0:T(4,128)} %param.27) | copy-start | bytes 196
  118.8 5.7 %copy-start.12 = (f32[4,4]{1,0:T(4,128)S(1)}, f32[4,4]{1,0:T(4,128)}, u32[]{:S(2)}) copy-start(f32[4,4]{1,0:T(4,128)} %param.28) | copy-start | bytes 196
  118.8 5.8 %copy-start.1 = (bf16[4,512,256]{1,2,0:T(8,128)(2,1)S(1)}, bf16[4,512,256]{1,2,0:T(8,128)(2,1)}, u32[]{:S(2)}) copy-start(bf16[4,512,256]{1,2,0:T(8,128)(2,1)} %copy.22) | copy-start | bytes 3145732
  123.1 20.3 %copy-start.10 = (bf16[4,4,16]{2,1,0:T(4,128)(2,1)S(1)}, bf16[4,4,16]{2,1,0:T(4,128)(2,1)}, u32[]{:S(2)}) copy-start(bf16[4,4,16]{2,1,0:T(4,128)(2,1)} %param.26) | copy-start | bytes 1540
  123.1 205.7 %reduce-scatter.8.cloned.1.call-start = ((), (), s32[]{:S(2)}) async-start(), calls=%async_computation.3 | async-start | bytes 2162688
Sparse Core Ops, SparseCore 0:
  123.3 61.9 reduce-scatter.5
  191.3 137.5 reduce-scatter.7
where the time goes:
time: 338 us; the launch traced here: 337 us
  waiting for transfers between devices  160 us (47%)
  blocking collectives  83.3 us (25%)
  matrix products  42.6 us (13%)
  local copies, waits for them, and re-layouts  17.5 us (5%)
  between operations  15 us (4%)
  other arithmetic  12.1 us (4%)
  starting transfers between devices  6.87 us (2%)
    unnamed x3, waiting for transfers between devices  137 us
    all_gather x1, blocking collectives, carried_in(): everything = lax.all_gather(shard, axis)  27 us
    reduce_scatter x1, waiting for transfers between devices, body(): lax.psum_scatter(memory_part, 'sp', scatter_dimension=3, tiled=True)  22.6 us
    pmax x1, blocking collectives, body(): peak_log = lax.pmax(jnp.max(gate_log, axis=1), 'sp')  19.5 us
    psum x1, blocking collectives, body(): denom = lax.psum(jnp.sum(query_slice * normer_next, axis=-1), 'sp')  19.2 us
    unnamed x1, blocking collectives  17.6 us
    dot_general x1, matrix products, project(): jnp.dot(flat_rows, value_weight, preferred_element_type=jnp.float32)  14.8 us
    convert_element_type x2, local copies, waits for them, and re-layouts, body(): weighted_rows = (value_four * scale[..., None]).astype(jnp.bfloat16)  10.5 us
  transfers between devices with their start and end apart: 4, of which 2 were waited for; matrix products, arithmetic and copies ran while one was open for 13% of the time, Pallas kernels for 0%

commit v1 on v0

v1 whole, which is shorter than its diff:
```python
import functools

import jax
import jax.numpy as jnp
from jax import lax
from jax.experimental import pallas as pl
from jax.experimental.pallas import tpu as pltpu
from jax.sharding import PartitionSpec as P

EDGE = 16
EXTRA_ROWS = 8


def log_sigmoid(x):
    return jnp.minimum(x, 0.0) - jnp.log1p(jnp.exp(-jnp.abs(x)))


def three_parts(x):
    high = x.astype(jnp.bfloat16)
    rest = x - high.astype(jnp.float32)
    middle = rest.astype(jnp.bfloat16)
    low = (rest - middle.astype(jnp.float32)).astype(jnp.bfloat16)
    return jnp.concatenate([high, middle, low], axis=1)


def kernel(
    sp_count,
    tp_count,
    prompt,
    key_weight,
    value_weight,
    out_weight,
    gate_weight,
    bias,
    taps,
    extra,
    small,
    new_value,
    memory_out,
    norm_out,
    peak_out,
    read_out,
    rows,
    edges,
    wk,
    wv,
    wo,
    later,
    padded,
    values,
    gates,
    share,
    shares,
    halo_out,
    halo_in,
    parts_out,
    parts_in,
    row_sem,
    edge_sem,
    weight_sem,
    share_send,
    share_recv,
    halo_send,
    halo_recv,
    part_send,
    part_recv,
):
    seqs, seg, width = rows.shape
    lanes = wk.shape[1]
    heads = bias.shape[1]
    key_size = lanes // heads
    value_size = wv.shape[1] // heads
    cols = value_size // sp_count
    total = sp_count * tp_count
    sp, tp = lax.axis_index("sp"), lax.axis_index("tp")
    me = sp * tp_count + tp
    f32, bf16 = jnp.float32, jnp.bfloat16

    def device(j):
        return {"sp": j // tp_count, "tp": lax.rem(j, tp_count)}

    barrier = pltpu.get_barrier_semaphore()

    def greet(o, carry):
        j = lax.rem(me + o, total)
        pl.semaphore_signal(
            barrier, inc=1, device_id=device(j), device_id_type=pl.DeviceIdType.MESH
        )
        return carry

    key_copy = pltpu.make_async_copy(key_weight, wk, weight_sem.at[0])
    value_copy = pltpu.make_async_copy(value_weight, wv, weight_sem.at[1])
    out_copy = pltpu.make_async_copy(out_weight, wo, weight_sem.at[2])
    edge_copies = [
        pltpu.make_async_copy(
            prompt.at[s, pl.ds(start, EDGE)], edges.at[2 * s + side], edge_sem.at[2 * s + side]
        )
        for s in range(seqs)
        for side, start in enumerate((0, seg - EDGE))
    ]
    key_copy.start()
    for copy in edge_copies:
        copy.start()
    pltpu.make_async_copy(prompt.at[0], rows.at[0], row_sem.at[0]).start()
    value_copy.start()
    for s in range(1, seqs):
        pltpu.make_async_copy(prompt.at[s], rows.at[s], row_sem.at[s]).start()
    out_copy.start()
    lax.fori_loop(1, total, greet, 0)

    place = lax.broadcasted_iota(jnp.int32, (seg, seg), 0)
    other = lax.broadcasted_iota(jnp.int32, (seg, seg), 1)
    later[...] = jnp.where(other > place, 1.0, 0.0).astype(bf16)

    for copy in edge_copies:
        copy.wait()
    key_copy.wait()
    edge_keys = jnp.dot(
        edges[...].reshape(2 * seqs * EDGE, width), wk[...], preferred_element_type=f32
    )
    edge_keys = edge_keys.astype(bf16).astype(f32)
    for s in range(seqs):
        first = 2 * s * EDGE
        last = first + 2 * EDGE - 1
        halo_out[0, s : s + 1, :] = edge_keys[last : last + 1]
        halo_out[1, s : s + 1, :] = edge_keys[first : first + 1]
    pl.semaphore_wait(barrier, total - 1)
    after = lax.rem(sp + 1, sp_count)
    before = lax.rem(sp + sp_count - 1, sp_count)
    halo_copies = [
        pltpu.make_async_remote_copy(
            src_ref=halo_out.at[i],
            dst_ref=halo_in.at[i],
            send_sem=halo_send.at[i],
            recv_sem=halo_recv.at[i],
            device_id={"sp": to, "tp": tp},
            device_id_type=pl.DeviceIdType.MESH,
        )
        for i, to in enumerate((after, before))
    ]
    for copy in halo_copies:
        copy.start()
    value_copy.wait()

    lane_head = lax.broadcasted_iota(jnp.int32, (1, lanes), 1) // key_size
    tap = taps[...].astype(f32)

    def by_head(x):
        out = jnp.zeros((x.shape[0], lanes), f32)
        for h in range(heads):
            out = jnp.where(lane_head == h, x[:, h : h + 1], out)
        return out

    def share_copy(s, q):
        return pltpu.make_async_remote_copy(
            src_ref=share.at[s, q],
            dst_ref=shares.at[s, sp],
            send_sem=share_send.at[s, q],
            recv_sem=share_recv.at[s, sp],
            device_id={"sp": q, "tp": tp},
            device_id_type=pl.DeviceIdType.MESH,
        )

    block = min(256, seg)

    def project(i, s):
        at = pl.ds(pl.multiple_of(i * block, block), block)
        x = rows[s, at, :]
        key_raw = jnp.dot(x, wk[...], preferred_element_type=f32)
        padded[pl.ds(pl.multiple_of(i * block + 8, 8), block), :] = key_raw.astype(bf16).astype(f32)
        values[at, :] = jnp.dot(x, wv[...], preferred_element_type=f32).astype(bf16)
        gate = jnp.dot(x, gate_weight[...], preferred_element_type=f32)
        gates[at, :] = gate.astype(bf16).astype(f32)
        return s

    def sequence(s, carry):
        pltpu.make_async_copy(prompt.at[s], rows.at[s], row_sem.at[s]).wait()
        lax.fori_loop(0, seg // block, project, s)

        @pl.when(s == 0)
        def _():
            for copy in halo_copies:
                copy.wait()

        zero = jnp.zeros((1, lanes), f32)
        padded[7:8, :] = jnp.where(sp == 0, zero, halo_in[0, pl.ds(s, 1), :])
        padded[seg + 8 : seg + 9, :] = jnp.where(
            sp == sp_count - 1, zero, halo_in[1, pl.ds(s, 1), :]
        )
        mixed = (
            tap[0:1] * padded[7 : seg + 7, :]
            + tap[1:2] * padded[8 : seg + 8, :]
            + tap[2:3] * padded[9 : seg + 9, :]
        )
        key_rows = (mixed * jax.nn.sigmoid(mixed) * key_size ** (-0.5)).astype(bf16)

        gate = gates[...]
        log_forget = log_sigmoid(gate[:, :heads] + bias[...]) + extra[s]
        sums = jnp.dot(later[...], three_parts(log_forget), preferred_element_type=f32)
        suffix = sums[:, :heads] + sums[:, heads : 2 * heads] + sums[:, 2 * heads :]
        gate_log = gate[:, heads:] + suffix
        seg_total = jnp.sum(log_forget, axis=0, keepdims=True)
        top = jnp.max(gate_log, axis=0, keepdims=True)
        scale = jnp.exp(gate_log - top)

        over = (((0,), (0,)), ((), ()))
        memory = jnp.zeros((value_size, lanes), f32)
        for h in range(heads):
            value = values[:, h * value_size : (h + 1) * value_size].astype(f32)
            weighted = (value * scale[:, h : h + 1]).astype(bf16)
            outer = lax.dot_general(weighted, key_rows, over, preferred_element_type=f32)
            memory = jnp.where(lane_head == h, outer, memory)
        normers = lax.dot_general(
            three_parts(scale), key_rows, over, preferred_element_type=f32
        )
        row_head = lax.rem(lax.broadcasted_iota(jnp.int32, normers.shape, 0), heads)
        normer = jnp.sum(jnp.where(row_head == lane_head, normers, 0.0), axis=0, keepdims=True)
        row = lax.broadcasted_iota(jnp.int32, (EXTRA_ROWS, lanes), 0)
        extras = jnp.where(row == 0, normer, jnp.where(row == 1, by_head(seg_total), by_head(top)))
        for q in range(sp_count):
            share[s, q, :cols, :] = memory[q * cols : (q + 1) * cols]
            share[s, q, cols:, :] = extras
        shares[s, sp] = share[s, sp]

        def send(o, c):
            share_copy(s, lax.rem(sp + o, sp_count)).start()
            return c

        return lax.fori_loop(1, sp_count, send, carry)

    lax.fori_loop(0, seqs, sequence, 0)
    out_copy.wait()

    def arrive(i, c):
        s = i // (sp_count - 1)
        q = lax.rem(sp + 1 + lax.rem(i, sp_count - 1), sp_count)
        pltpu.make_async_remote_copy(
            src_ref=share.at[s, q],
            dst_ref=shares.at[s, q],
            send_sem=share_send.at[s, q],
            recv_sem=share_recv.at[s, q],
            device_id={"sp": q, "tp": tp},
            device_id_type=pl.DeviceIdType.MESH,
        ).wait()
        return c

    lax.fori_loop(0, seqs * (sp_count - 1), arrive, 0)

    depth = heads * cols
    lane = lax.broadcasted_iota(jnp.int32, (depth, 128), 1)
    reads = jnp.zeros((depth, 128), f32)
    for s in range(seqs):
        pieces = [shares[s, d] for d in range(sp_count)]
        tail = jnp.zeros((1, lanes), f32)
        tops = [None] * sp_count
        for d in reversed(range(sp_count)):
            tops[d] = pieces[d][cols + 2 : cols + 3] + tail
            tail = tail + pieces[d][cols + 1 : cols + 2]
        peak = functools.reduce(jnp.maximum, tops)
        memory = jnp.zeros((cols, lanes), f32)
        normer = jnp.zeros((1, lanes), f32)
        for d in range(sp_count):
            factor = jnp.exp(tops[d] - peak)
            memory = memory + factor * pieces[d][:cols]
            normer = normer + factor * pieces[d][cols : cols + 1]
        memory_out[s] = memory
        norm_out[s : s + 1, :] = normer
        peak_out[s : s + 1, :] = peak
        query, key = small[0, s : s + 1, :], small[1, s : s + 1, :]
        input_new, forget_new = small[2, s : s + 1, :], log_sigmoid(small[3, s : s + 1, :])
        new_peak = jnp.maximum(forget_new + peak, input_new)
        old_scale = jnp.exp(forget_new + peak - new_peak)
        new_scale = jnp.exp(input_new - new_peak)
        numer = query * (old_scale * memory + new_scale * key * new_value[s])
        denom = query * (old_scale * normer + new_scale * key)
        found = []
        for h in range(heads):
            top = jnp.sum(jnp.where(lane_head == h, numer, 0.0), axis=1, keepdims=True)
            under = jnp.sum(jnp.where(lane_head == h, denom, 0.0), axis=1, keepdims=True)
            found.append(top / jnp.maximum(jnp.abs(under), 1.0))
        reads = jnp.where(lane == s, jnp.concatenate(found, axis=0), reads)
    if depth < 128:
        reads = jnp.concatenate([reads, jnp.zeros((128 - depth, 128), f32)], axis=0)
    left = reads.T[:8, :depth].astype(bf16)
    partial = jnp.dot(left, wo[...], preferred_element_type=f32)
    features = read_out.shape[1]
    for j in range(total):
        parts_out[j] = partial[:seqs, j * features : (j + 1) * features]
    parts_in[me] = parts_out[me]

    def part_copy(j, slot):
        return pltpu.make_async_remote_copy(
            src_ref=parts_out.at[j],
            dst_ref=parts_in.at[slot],
            send_sem=part_send.at[j],
            recv_sem=part_recv.at[slot],
            device_id=device(j),
            device_id_type=pl.DeviceIdType.MESH,
        )

    def send_part(o, c):
        part_copy(lax.rem(me + o, total), me).start()
        return c

    def take_part(o, c):
        j = lax.rem(me + o, total)
        part_copy(j, j).wait()
        return c

    lax.fori_loop(1, total, send_part, 0)
    lax.fori_loop(1, total, take_part, 0)
    read_out[...] = jnp.sum(parts_in[...], axis=0).astype(bf16)


def body(
    prompt,
    key_weight,
    value_weight,
    input_gate_weight,
    forget_gate_weight,
    forget_bias,
    key_taps,
    extra_decay,
    new_query,
    new_key,
    new_value,
    new_input_gate,
    new_forget_gate,
    out_weight,
):
    f32, bf16 = jnp.float32, jnp.bfloat16
    sp_count, tp_count = lax.axis_size("sp"), lax.axis_size("tp")
    total = sp_count * tp_count
    seqs, seg, width = prompt.shape
    heads, key_size = new_key.shape[1:]
    lanes = heads * key_size
    cols = new_value.shape[2]
    value_width = value_weight.shape[1]
    depth = heads * cols
    out_width = out_weight.shape[2]
    features = out_width // total

    def by_lane(x):
        return jnp.repeat(x.astype(f32), key_size, axis=-1)

    small = jnp.stack(
        [
            new_query.reshape(seqs, lanes).astype(f32),
            new_key.reshape(seqs, lanes).astype(f32),
            by_lane(new_input_gate),
            by_lane(new_forget_gate),
        ]
    )
    value_lanes = by_lane(new_value.transpose(0, 2, 1))
    gate_weight = jnp.concatenate([forget_gate_weight, input_gate_weight], axis=1)
    vmem = pl.BlockSpec(memory_space=pltpu.VMEM)
    hbm = pl.BlockSpec(memory_space=pl.ANY)
    block_rows = cols + EXTRA_ROWS
    memory, normer, peak, read = pl.pallas_call(
        functools.partial(kernel, sp_count, tp_count),
        out_shape=(
            jax.ShapeDtypeStruct((seqs, cols, lanes), f32),
            jax.ShapeDtypeStruct((seqs, lanes), f32),
            jax.ShapeDtypeStruct((seqs, lanes), f32),
            jax.ShapeDtypeStruct((seqs, features), bf16),
        ),
        in_specs=[hbm] * 4 + [vmem] * 6,
        out_specs=[vmem] * 4,
        scratch_shapes=[
            pltpu.VMEM((seqs, seg, width), bf16),
            pltpu.VMEM((2 * seqs, EDGE, width), bf16),
            pltpu.VMEM((width, lanes), bf16),
            pltpu.VMEM((width, value_width), bf16),
            pltpu.VMEM((depth, out_width), bf16),
            pltpu.VMEM((seg, seg), bf16),
            pltpu.VMEM((seg + 16, lanes), f32),
            pltpu.VMEM((seg, value_width), bf16),
            pltpu.VMEM((seg, 2 * heads), f32),
            pltpu.VMEM((seqs, sp_count, block_rows, lanes), f32),
            pltpu.VMEM((seqs, sp_count, block_rows, lanes), f32),
            pltpu.VMEM((2, seqs, lanes), f32),
            pltpu.VMEM((2, seqs, lanes), f32),
            pltpu.VMEM((total, seqs, features), f32),
            pltpu.VMEM((total, seqs, features), f32),
            pltpu.SemaphoreType.DMA((seqs,)),
            pltpu.SemaphoreType.DMA((2 * seqs,)),
            pltpu.SemaphoreType.DMA((3,)),
            pltpu.SemaphoreType.DMA((seqs, sp_count)),
            pltpu.SemaphoreType.DMA((seqs, sp_count)),
            pltpu.SemaphoreType.DMA((2,)),
            pltpu.SemaphoreType.DMA((2,)),
            pltpu.SemaphoreType.DMA((total,)),
            pltpu.SemaphoreType.DMA((total,)),
        ],
        compiler_params=pltpu.CompilerParams(
            collective_id=0, has_side_effects=True, vmem_limit_bytes=60 * 2**20
        ),
    )(
        prompt,
        key_weight,
        value_weight,
        out_weight.reshape(depth, out_width),
        gate_weight,
        forget_bias.reshape(1, heads),
        key_taps,
        extra_decay,
        small,
        value_lanes,
    )
    memory = memory.reshape(seqs, cols, heads, key_size).transpose(0, 2, 3, 1)
    key_cols = key_size // sp_count
    normer = lax.dynamic_slice_in_dim(
        normer.reshape(seqs, heads, key_size), lax.axis_index("sp") * key_cols, key_cols, 2
    )
    return (
        memory.astype(bf16),
        normer.astype(bf16),
        peak.reshape(seqs, heads, key_size)[:, :, 0],
        read,
    )


def solution(mesh):
    placed = (
        P(None, "sp", None),
        P(None, "tp"),
        P(None, "tp"),
        P(None, "tp"),
        P(None, "tp"),
        P("tp"),
        P(None, "tp"),
        P(None, "sp", "tp"),
        P(None, "tp", None),
        P(None, "tp", None),
        P(None, "tp", "sp"),
        P(None, "tp"),
        P(None, "tp"),
        P("tp", "sp", None),
    )
    return jax.shard_map(
        body,
        mesh=mesh,
        in_specs=placed,
        out_specs=(
            P(None, "tp", None, "sp"),
            P(None, "tp", "sp"),
            P(None, "tp"),
            P(None, ("sp", "tp")),
        ),
        check_vma=False,
    )
```

time: 338 us -> 68.5 us (0.20)
  waiting for transfers between devices: 160 us -> 0 us
  blocking collectives: 83.3 us -> 0 us
  Pallas kernels: 0 us -> 51.8 us
  matrix products: 42.6 us -> 0 us
  between operations: 15 us -> 0.67 us
  other arithmetic: 12.1 us -> 2.95 us
  starting transfers between devices: 6.87 us -> 0 us
  local copies, waits for them, and re-layouts: 17.5 us -> 12.5 us
    unnamed x3 -> x0, waiting for transfers between devices: 137 us -> none
    pallas_call x0 -> x1, Pallas kernels: none -> 51.8 us  [body(): pl.pallas_call(functools.partial(kernel, sp_count, tp_count), out_shape=(...]
    dot_general x6 -> x0, matrix products: 42.6 us -> none  [the longest x1 14.8 us: project(): jnp.dot(flat_rows, value_weight, preferred_element_type=jnp.float32)]
    all_gather x1 -> x0, blocking collectives: 27 us -> none  [carried_in(): everything = lax.all_gather(shard, axis)]
    reduce_scatter x1 -> x0, waiting for transfers between devices: 22.6 us -> none  [body(): lax.psum_scatter(memory_part, 'sp', scatter_dimension=3, tiled=True)]
    pmax x1 -> x0, blocking collectives: 19.5 us -> none  [body(): peak_log = lax.pmax(jnp.max(gate_log, axis=1), 'sp')]
    psum x1 -> x0, blocking collectives: 19.2 us -> none  [body(): denom = lax.psum(jnp.sum(query_slice * normer_next, axis=-1), 'sp')]
    unnamed x1 -> x0, blocking collectives: 17.6 us -> none
  transfers between devices with their start and end apart: 4 -> 0, of which waited for: 2 -> 0; matrix products, arithmetic and copies ran while one was open for 13% -> 0% of each run, Pallas kernels for 0% -> 0%
where the time goes in v1:
time: 68.5 us; the launch traced here: 68 us
  Pallas kernels  51.8 us (76%)
  local copies, waits for them, and re-layouts  12.5 us (18%)
  other arithmetic  2.95 us (4%)
    pallas_call x1, Pallas kernels, body(): pl.pallas_call(functools.partial(kernel, sp_count, tp_count), out_shape=(...  51.8 us
    unnamed x3, local copies, waits for them, and re-layouts  4.08 us
    broadcast_in_dim x3, local copies, waits for them, and re-layouts, by_lane(): return jnp.repeat(x.astype(f32), key_size, axis=-1)  1.63 us

profile of v1, /device:TPU:0, one launch (start us, length us, event | category | flops | bytes accessed | tf_op | source)
XLA Modules:
  0.0 68.0 jit_solution(8237306175661840701)
XLA Ops:
  0.6 0.8 %reshape.56 = f32[1,4,256]{2,1,0:T(4,128)S(1)} reshape(bf16[4,4,64]{2,1,0:T(4,128)(2,1)} %param.22) | data formatting | bytes 6144 | tf_op jit(solution)/shard_map/convert_element_type | solution.py:348
  1.4 0.8 %reshape.57 = f32[1,4,256]{2,1,0:T(4,128)S(1)} reshape(bf16[4,4,64]{2,1,0:T(4,128)(2,1)} %param.23) | data formatting | bytes 6144 | tf_op jit(solution)/shard_map/convert_element_type | solution.py:349
  2.2 0.7 %convert_bitcast_fusion = f32[4,16,4]{1,2,0:T(4,128)S(1)} fusion(bf16[4,4,16]{2,1,0:T(4,128)(2,1)} %param.24), kind=kLoop, calls=%fused_computation.3 | loop fusion | flops 256 | bytes 1536 | tf_op jit(solution)/shard_map/convert_element_type | solution.py:344
  2.9 0.8 %broadcast_in_dim.9 = f32[4,4,64]{2,1,0:T(4,128)S(1)} broadcast(f32[4,4]{1,0:T(4,128)} %param.25), dimensions={0,1} | broadcast | bytes 4160 | tf_op jit(solution)/shard_map/broadcast_in_dim | solution.py:344
  3.6 0.1 stack_reshape.6
  3.7 0.8 %broadcast_in_dim.10 = f32[4,4,64]{2,1,0:T(4,128)S(1)} broadcast(f32[4,4]{1,0:T(4,128)} %param.26), dimensions={0,1} | broadcast | bytes 4160 | tf_op jit(solution)/shard_map/broadcast_in_dim | solution.py:344
  4.5 0.1 stack_reshape.7
  4.5 0.6 pad_maximum_fusion.1.small
  5.1 0.1 copy.24
  5.2 0.8 %pad_maximum_fusion = bf16[4096,8]{0,1:T(8,128)(2,1)S(1)} fusion(bf16[4096,4]{0,1:T(4,128)(2,1)} %param.17, bf16[4096,4]{0,1:T(4,128)(2,1)} %param.18), kind=kLoop, calls=%fused_computation | loop fusion | flops 131072 | bytes 131072 | tf_op jit(solution)/shard_map/concatenate | solution.py:355
  6.1 0.1 broadcast_in_dim.11
  6.2 0.8 %reshape.53.new_value = f32[4,16,256]{2,1,0:T(8,128)} reshape(f32[4,16,4,64]{3,2,1,0:T(4,128)S(1)} %broadcast_in_dim.11) | data formatting | bytes 131072 | tf_op jit(solution)/shard_map/reshape | solution.py:344
  7.0 1.3 %copy.25.gate_weight = bf16[4096,8]{1,0:T(8,128)(2,1)} copy(bf16[4096,8]{0,1:T(8,128)(2,1)S(1)} %pad_maximum_fusion) | data formatting | bytes 131072 | tf_op jit(solution)/shard_map/concatenate | solution.py:355
  8.3 2.2 %copy.26.extra = f32[4,512,4]{2,1,0:T(8,128)} copy(f32[4,512,4]{1,2,0:T(4,128)} %param.21) | data formatting | bytes 65536 | tf_op args[7]
  10.4 51.8 %shard_map.165 = (f32[4,16,256]{2,1,0:T(8,128)}, f32[4,256]{1,0:T(4,128)}, f32[4,256]{1,0:T(4,128)}, bf16[4,128]{1,0:T(4,128)(2,1)}) custom-call(bf16[4,512,4096]{2,1,0:T(8,128)(2,1)} %prompt.1, bf16[4096,256]{1,0:T(8,128)(2,1)} %key_weight.1, bf16[4096,512]{1,0:T(8,128)(2,1)} %value_weight.1, bf16[64,4096]{1,0:T(8,128)(2,1)} %bitcast.9, ...), custom_call_target="tpu_custom_call" | custom-call | tf_op jit(solution)/shard_map/pallas_call | solution.py:359
  62.3 0.8 %convert_element_type.50 = bf16[4,16,256]{2,1,0:T(8,128)(2,1)S(1)} convert(f32[4,16,256]{2,1,0:T(8,128)} %get-tuple-element.8) | non-fusion elementwise | flops 16384 | bytes 98304 | tf_op jit(solution)/shard_map/convert_element_type | solution.py:416
  63.1 0.8 %reshape.54 = bf16[4,4,64]{2,1,0:T(4,128)(2,1)S(1)} reshape(f32[4,256]{1,0:T(4,128)} %get-tuple-element.9) | data formatting | bytes 6144 | tf_op jit(solution)/shard_map/reshape | solution.py:413
  63.9 0.7 dynamic-slice_convert_fusion
  64.5 0.8 %reshape.55 = f32[4,4,64]{2,1,0:T(4,128)S(1)} reshape(f32[4,256]{1,0:T(4,128)} %get-tuple-element.10) | data formatting | bytes 8192 | tf_op jit(solution)/shard_map/reshape | solution.py:418
  65.3 0.7 %copy.29 = f32[4,4,1]{1,0,2:T(4,128)} copy(f32[4,4,1]{2,1,0:T(4,128)S(1)} %bitcast.11) | data formatting | bytes 128
  66.0 0.1 convert_element_type.51
  66.1 0.6 copy.31
  66.7 1.2 %copy.33 = bf16[4,128]{1,0:T(4,128)(2,1)} copy(bf16[4,128]{1,0:T(4,128)(2,1)} %get-tuple-element.19) | data formatting | bytes 2048

commit v2 on v1

--- a/solution.py
+++ b/solution.py
@@ -8,7 +8,7 @@
 from jax.sharding import PartitionSpec as P
 
 EDGE = 16
-EXTRA_ROWS = 8
+NOTE_ROWS = 4
 
 
 def log_sigmoid(x):
@@ -16,11 +16,10 @@
 
 
 def three_parts(x):
-    high = x.astype(jnp.bfloat16)
-    rest = x - high.astype(jnp.float32)
-    middle = rest.astype(jnp.bfloat16)
-    low = (rest - middle.astype(jnp.float32)).astype(jnp.bfloat16)
-    return jnp.concatenate([high, middle, low], axis=1)
+    high = x.astype(jnp.bfloat16).astype(jnp.float32)
+    rest = x - high
+    middle = rest.astype(jnp.bfloat16).astype(jnp.float32)
+    return jnp.concatenate([high, middle, rest - middle], axis=0).astype(jnp.bfloat16)
 
 
 def kernel(
@@ -30,12 +29,16 @@
     key_weight,
     value_weight,
     out_weight,
-    gate_weight,
+    input_weight,
+    forget_weight,
     bias,
     taps,
     extra,
-    small,
+    new_query,
+    new_key,
     new_value,
+    new_input,
+    new_forget,
     memory_out,
     norm_out,
     peak_out,
@@ -45,12 +48,15 @@
     wk,
     wv,
     wo,
+    wg,
     later,
     padded,
     values,
     gates,
     share,
     shares,
+    note,
+    notes,
     halo_out,
     halo_in,
     parts_out,
@@ -60,6 +66,8 @@
     weight_sem,
     share_send,
     share_recv,
+    note_send,
+    note_recv,
     halo_send,
     halo_recv,
     part_send,
@@ -110,7 +118,19 @@
 
     place = lax.broadcasted_iota(jnp.int32, (seg, seg), 0)
     other = lax.broadcasted_iota(jnp.int32, (seg, seg), 1)
-    later[...] = jnp.where(other > place, 1.0, 0.0).astype(bf16)
+    later[...] = jnp.where(place > other, 1.0, 0.0).astype(bf16)
+    gate_rows = jnp.concatenate(
+        [forget_weight[...].astype(f32), input_weight[...].astype(f32)], axis=0
+    )
+    wg[...] = gate_rows.T.astype(bf16)
+
+    def column(x):
+        size = x.shape[1]
+        down = lax.broadcasted_iota(jnp.int32, (size, size), 0)
+        across = lax.broadcasted_iota(jnp.int32, (size, size), 1)
+        return jnp.sum(jnp.where(down == across, x, 0.0), axis=1, keepdims=True)
+
+    bias_column = column(bias[...])
 
     for copy in edge_copies:
         copy.wait()
@@ -151,12 +171,26 @@
             out = jnp.where(lane_head == h, x[:, h : h + 1], out)
         return out
 
-    def share_copy(s, q):
+    def columns_by_head(x):
+        row = lax.broadcasted_iota(jnp.int32, (heads, lanes), 0)
+        return jnp.sum(jnp.where(row == lane_head, x, 0.0), axis=0, keepdims=True)
+
+    def share_copy(s, q, slot):
         return pltpu.make_async_remote_copy(
             src_ref=share.at[s, q],
-            dst_ref=shares.at[s, sp],
+            dst_ref=shares.at[s, slot],
             send_sem=share_send.at[s, q],
-            recv_sem=share_recv.at[s, sp],
+            recv_sem=share_recv.at[s, slot],
+            device_id={"sp": q, "tp": tp},
+            device_id_type=pl.DeviceIdType.MESH,
+        )
+
+    def note_copy(s, q, slot):
+        return pltpu.make_async_remote_copy(
+            src_ref=note.at[s],
+            dst_ref=notes.at[s, slot],
+            send_sem=note_send.at[s, q],
+            recv_sem=note_recv.at[s, slot],
             device_id={"sp": q, "tp": tp},
             device_id_type=pl.DeviceIdType.MESH,
         )
@@ -169,8 +203,8 @@
         key_raw = jnp.dot(x, wk[...], preferred_element_type=f32)
         padded[pl.ds(pl.multiple_of(i * block + 8, 8), block), :] = key_raw.astype(bf16).astype(f32)
         values[at, :] = jnp.dot(x, wv[...], preferred_element_type=f32).astype(bf16)
-        gate = jnp.dot(x, gate_weight[...], preferred_element_type=f32)
-        gates[at, :] = gate.astype(bf16).astype(f32)
+        gate = jnp.dot(x, wg[...], preferred_element_type=f32)
+        gates[:, at] = gate.T.astype(bf16).astype(f32)
         return s
 
     def sequence(s, carry):
@@ -195,35 +229,38 @@
         key_rows = (mixed * jax.nn.sigmoid(mixed) * key_size ** (-0.5)).astype(bf16)
 
         gate = gates[...]
-        log_forget = log_sigmoid(gate[:, :heads] + bias[...]) + extra[s]
-        sums = jnp.dot(later[...], three_parts(log_forget), preferred_element_type=f32)
-        suffix = sums[:, :heads] + sums[:, heads : 2 * heads] + sums[:, 2 * heads :]
-        gate_log = gate[:, heads:] + suffix
-        seg_total = jnp.sum(log_forget, axis=0, keepdims=True)
-        top = jnp.max(gate_log, axis=0, keepdims=True)
+        log_forget = log_sigmoid(gate[:heads] + bias_column) + extra[s]
+        sums = jnp.dot(three_parts(log_forget), later[...], preferred_element_type=f32)
+        suffix = sums[:heads] + sums[heads : 2 * heads] + sums[2 * heads :]
+        gate_log = gate[heads:] + suffix
+        seg_total = jnp.sum(log_forget, axis=1, keepdims=True)
+        top = jnp.max(gate_log, axis=1, keepdims=True)
         scale = jnp.exp(gate_log - top)
+        scale_columns = jnp.concatenate([scale, jnp.zeros((8 - heads, seg), f32)], axis=0).T
 
         over = (((0,), (0,)), ((), ()))
         memory = jnp.zeros((value_size, lanes), f32)
         for h in range(heads):
             value = values[:, h * value_size : (h + 1) * value_size].astype(f32)
-            weighted = (value * scale[:, h : h + 1]).astype(bf16)
+            weighted = (value * scale_columns[:, h : h + 1]).astype(bf16)
             outer = lax.dot_general(weighted, key_rows, over, preferred_element_type=f32)
             memory = jnp.where(lane_head == h, outer, memory)
-        normers = lax.dot_general(
-            three_parts(scale), key_rows, over, preferred_element_type=f32
-        )
+        normers = jnp.dot(three_parts(scale), key_rows, preferred_element_type=f32)
         row_head = lax.rem(lax.broadcasted_iota(jnp.int32, normers.shape, 0), heads)
         normer = jnp.sum(jnp.where(row_head == lane_head, normers, 0.0), axis=0, keepdims=True)
-        row = lax.broadcasted_iota(jnp.int32, (EXTRA_ROWS, lanes), 0)
-        extras = jnp.where(row == 0, normer, jnp.where(row == 1, by_head(seg_total), by_head(top)))
+        note[s, 0:1, :] = normer
+        note[s, 1:2, :] = columns_by_head(seg_total)
+        note[s, 2:3, :] = columns_by_head(top)
+        note[s, 3:4, :] = jnp.zeros((1, lanes), f32)
         for q in range(sp_count):
-            share[s, q, :cols, :] = memory[q * cols : (q + 1) * cols]
-            share[s, q, cols:, :] = extras
+            share[s, q] = memory[q * cols : (q + 1) * cols].astype(bf16)
         shares[s, sp] = share[s, sp]
+        notes[s, sp] = note[s]
 
         def send(o, c):
-            share_copy(s, lax.rem(sp + o, sp_count)).start()
+            q = lax.rem(sp + o, sp_count)
+            note_copy(s, q, sp).start()
+            share_copy(s, q, sp).start()
             return c
 
         return lax.fori_loop(1, sp_count, send, carry)
@@ -234,15 +271,22 @@
     def arrive(i, c):
         s = i // (sp_count - 1)
         q = lax.rem(sp + 1 + lax.rem(i, sp_count - 1), sp_count)
-        pltpu.make_async_remote_copy(
-            src_ref=share.at[s, q],
-            dst_ref=shares.at[s, q],
-            send_sem=share_send.at[s, q],
-            recv_sem=share_recv.at[s, q],
-            device_id={"sp": q, "tp": tp},
-            device_id_type=pl.DeviceIdType.MESH,
-        ).wait()
+        note_copy(s, q, q).wait()
+        share_copy(s, q, q).wait()
         return c
+
+    queries, keys = (
+        jnp.concatenate([ref[:, h, :].astype(f32) for h in range(heads)], axis=1)
+        for ref in (new_query, new_key)
+    )
+    inputs = [by_head(new_input[s : s + 1, :]) for s in range(seqs)]
+    forgets = [log_sigmoid(by_head(new_forget[s : s + 1, :])) for s in range(seqs)]
+    fresh = []
+    for s in range(seqs):
+        out = jnp.zeros((cols, lanes), f32)
+        for h in range(heads):
+            out = jnp.where(lane_head == h, column(new_value[s, h : h + 1, :].astype(f32)), out)
+        fresh.append(out)
 
     lax.fori_loop(0, seqs * (sp_count - 1), arrive, 0)
 
@@ -250,28 +294,33 @@
     lane = lax.broadcasted_iota(jnp.int32, (depth, 128), 1)
     reads = jnp.zeros((depth, 128), f32)
     for s in range(seqs):
-        pieces = [shares[s, d] for d in range(sp_count)]
         tail = jnp.zeros((1, lanes), f32)
         tops = [None] * sp_count
         for d in reversed(range(sp_count)):
-            tops[d] = pieces[d][cols + 2 : cols + 3] + tail
-            tail = tail + pieces[d][cols + 1 : cols + 2]
+            tops[d] = notes[s, d, 2:3, :] + tail
+            tail = tail + notes[s, d, 1:2, :]
         peak = functools.reduce(jnp.maximum, tops)
         memory = jnp.zeros((cols, lanes), f32)
         normer = jnp.zeros((1, lanes), f32)
         for d in range(sp_count):
             factor = jnp.exp(tops[d] - peak)
-            memory = memory + factor * pieces[d][:cols]
-            normer = normer + factor * pieces[d][cols : cols + 1]
-        memory_out[s] = memory
-        norm_out[s : s + 1, :] = normer
-        peak_out[s : s + 1, :] = peak
-        query, key = small[0, s : s + 1, :], small[1, s : s + 1, :]
-        input_new, forget_new = small[2, s : s + 1, :], log_sigmoid(small[3, s : s + 1, :])
+            memory = memory + factor * shares[s, d].astype(f32)
+            normer = normer + factor * notes[s, d, 0:1, :]
+        key_cols = norm_out.shape[2]
+        turned = pltpu.roll(
+            jnp.broadcast_to(normer, (8, lanes)), lax.rem(lanes - sp * key_cols, lanes), 1
+        )
+        for h in range(heads):
+            start = h * key_size
+            memory_out[s, h] = memory[:, start : start + key_size]
+            norm_out[s, h : h + 1, :] = turned[0:1, start : start + key_cols]
+            peak_out[s : s + 1, h : h + 1] = peak[:, start : start + 1]
+        query, key = queries[s : s + 1], keys[s : s + 1]
+        input_new, forget_new = inputs[s], forgets[s]
         new_peak = jnp.maximum(forget_new + peak, input_new)
         old_scale = jnp.exp(forget_new + peak - new_peak)
         new_scale = jnp.exp(input_new - new_peak)
-        numer = query * (old_scale * memory + new_scale * key * new_value[s])
+        numer = query * (old_scale * memory + new_scale * key * fresh[s])
         denom = query * (old_scale * normer + new_scale * key)
         found = []
         for h in range(heads):
@@ -340,31 +389,17 @@
     out_width = out_weight.shape[2]
     features = out_width // total
 
-    def by_lane(x):
-        return jnp.repeat(x.astype(f32), key_size, axis=-1)
-
-    small = jnp.stack(
-        [
-            new_query.reshape(seqs, lanes).astype(f32),
-            new_key.reshape(seqs, lanes).astype(f32),
-            by_lane(new_input_gate),
-            by_lane(new_forget_gate),
-        ]
-    )
-    value_lanes = by_lane(new_value.transpose(0, 2, 1))
-    gate_weight = jnp.concatenate([forget_gate_weight, input_gate_weight], axis=1)
     vmem = pl.BlockSpec(memory_space=pltpu.VMEM)
     hbm = pl.BlockSpec(memory_space=pl.ANY)
-    block_rows = cols + EXTRA_ROWS
     memory, normer, peak, read = pl.pallas_call(
         functools.partial(kernel, sp_count, tp_count),
         out_shape=(
-            jax.ShapeDtypeStruct((seqs, cols, lanes), f32),
-            jax.ShapeDtypeStruct((seqs, lanes), f32),
-            jax.ShapeDtypeStruct((seqs, lanes), f32),
+            jax.ShapeDtypeStruct((seqs, heads, cols, key_size), f32),
+            jax.ShapeDtypeStruct((seqs, heads, key_size // sp_count), f32),
+            jax.ShapeDtypeStruct((seqs, heads), f32),
             jax.ShapeDtypeStruct((seqs, features), bf16),
         ),
-        in_specs=[hbm] * 4 + [vmem] * 6,
+        in_specs=[hbm] * 4 + [vmem] * 10,
         out_specs=[vmem] * 4,
         scratch_shapes=[
             pltpu.VMEM((seqs, seg, width), bf16),
@@ -372,12 +407,15 @@
             pltpu.VMEM((width, lanes), bf16),
             pltpu.VMEM((width, value_width), bf16),
             pltpu.VMEM((depth, out_width), bf16),
+            pltpu.VMEM((width, 2 * heads), bf16),
             pltpu.VMEM((seg, seg), bf16),
             pltpu.VMEM((seg + 16, lanes), f32),
             pltpu.VMEM((seg, value_width), bf16),
-            pltpu.VMEM((seg, 2 * heads), f32),
-            pltpu.VMEM((seqs, sp_count, block_rows, lanes), f32),
-            pltpu.VMEM((seqs, sp_count, block_rows, lanes), f32),
+            pltpu.VMEM((2 * heads, seg), f32),
+            pltpu.VMEM((seqs, sp_count, cols, lanes), bf16),
+            pltpu.VMEM((seqs, sp_count, cols, lanes), bf16),
+            pltpu.VMEM((seqs, NOTE_ROWS, lanes), f32),
+            pltpu.VMEM((seqs, sp_count, NOTE_ROWS, lanes), f32),
             pltpu.VMEM((2, seqs, lanes), f32),
             pltpu.VMEM((2, seqs, lanes), f32),
             pltpu.VMEM((total, seqs, features), f32),
@@ -385,6 +423,8 @@
             pltpu.SemaphoreType.DMA((seqs,)),
             pltpu.SemaphoreType.DMA((2 * seqs,)),
             pltpu.SemaphoreType.DMA((3,)),
+            pltpu.SemaphoreType.DMA((seqs, sp_count)),
+            pltpu.SemaphoreType.DMA((seqs, sp_count)),
             pltpu.SemaphoreType.DMA((seqs, sp_count)),
             pltpu.SemaphoreType.DMA((seqs, sp_count)),
             pltpu.SemaphoreType.DMA((2,)),
@@ -400,24 +440,18 @@
         key_weight,
         value_weight,
         out_weight.reshape(depth, out_width),
-        gate_weight,
+        input_gate_weight.T,
+        forget_gate_weight.T,
         forget_bias.reshape(1, heads),
         key_taps,
-        extra_decay,
-        small,
-        value_lanes,
-    )
-    memory = memory.reshape(seqs, cols, heads, key_size).transpose(0, 2, 3, 1)
-    key_cols = key_size // sp_count
-    normer = lax.dynamic_slice_in_dim(
-        normer.reshape(seqs, heads, key_size), lax.axis_index("sp") * key_cols, key_cols, 2
-    )
-    return (
-        memory.astype(bf16),
-        normer.astype(bf16),
-        peak.reshape(seqs, heads, key_size)[:, :, 0],
-        read,
-    )
+        extra_decay.transpose(0, 2, 1),
+        new_query,
+        new_key,
+        new_value,
+        new_input_gate,
+        new_forget_gate,
+    )
+    return (memory.transpose(0, 1, 3, 2).astype(bf16), normer.astype(bf16), peak, read)
 
 
 def solution(mesh):

time: 68.5 us -> 54.5 us (0.80)
  local copies, waits for them, and re-layouts: 12.5 us -> 2.43 us
  Pallas kernels: 51.8 us -> 48.3 us
    pallas_call x1, Pallas kernels: 51.8 us -> 48.3 us  [body(): pl.pallas_call(functools.partial(kernel, sp_count, tp_count), out_shape=(...]
    convert_element_type x6 -> x0, local copies, waits for them, and re-layouts: 3.05 us -> none  [the longest x1 0.77 us: body(): new_query.reshape(seqs, lanes).astype(f32)]
    reshape x3 -> x0, local copies, waits for them, and re-layouts: 2.28 us -> none  [the longest x1 0.77 us: body(): normer.reshape(seqs, heads, key_size)]
    unnamed x3 -> x2, local copies, waits for them, and re-layouts: 4.08 us -> 2.43 us
    broadcast_in_dim x3 -> x0, local copies, waits for them, and re-layouts: 1.63 us -> none  [by_lane(): return jnp.repeat(x.astype(f32), key_size, axis=-1)]
    concatenate x1 -> x0, local copies, waits for them, and re-layouts: 1.33 us -> none  [body(): jnp.concatenate([forget_gate_weight, input_gate_weight], axis=1)]
    convert_element_type x2, other arithmetic: 1.54 us -> 2.84 us  [the longest x1 1.54 us: body(): memory.transpose(0, 1, 3, 2).astype(bf16)]
    concatenate x1 -> x0, other arithmetic: 0.81 us -> none  [body(): jnp.concatenate([forget_gate_weight, input_gate_weight], axis=1)]
where the time goes in v2:
time: 54.5 us; the launch traced here: 54.2 us
  Pallas kernels  48.3 us (89%)
  other arithmetic  2.84 us (5%)
  local copies, waits for them, and re-layouts  2.43 us (4%)
  between operations  0.65 us (1%)
    pallas_call x1, Pallas kernels, body(): pl.pallas_call(functools.partial(kernel, sp_count, tp_count), out_shape=(...  48.3 us
    unnamed x2, local copies, waits for them, and re-layouts  2.43 us
    convert_element_type x1, other arithmetic, body(): memory.transpose(0, 1, 3, 2).astype(bf16)  1.54 us
    convert_element_type x1, other arithmetic, body(): normer.astype(bf16)  1.29 us

profile of v2, /device:TPU:0, one launch (start us, length us, event | category | flops | bytes accessed | tf_op | source)
XLA Modules:
  0.0 54.2 jit_solution(4389687664370762373)
XLA Ops:
  0.6 48.3 %shard_map.165 = (f32[4,4,16,64]{3,2,1,0:T(8,128)}, f32[4,4,8]{2,1,0:T(4,128)}, f32[4,4]{1,0:T(4,128)}, bf16[4,128]{1,0:T(4,128)(2,1)}) custom-call(bf16[4,512,4096]{2,1,0:T(8,128)(2,1)} %prompt.1, bf16[4096,256]{1,0:T(8,128)(2,1)} %key_weight.1, bf16[4096,512]{1,0:T(8,128)(2,1)} %value_weight.1, bf16[64,4096]{1,0:T(8,128)(2,1)} %bitcast.7, ...), custom_call_target="tpu_custom_call" | custom-call | tf_op jit(solution)/shard_map/pallas_call | solution.py:394
  48.9 1.5 %convert_bitcast_fusion = bf16[4,4,64,16]{2,3,1,0:T(8,128)(2,1)} fusion(f32[4,4,16,64]{3,2,1,0:T(8,128)} %get-tuple-element.8), kind=kLoop, calls=%fused_computation | loop fusion | flops 16384 | bytes 98304 | tf_op jit(solution)/shard_map/convert_element_type | solution.py:454
  50.5 1.3 %convert_element_type.11 = bf16[4,4,8]{2,1,0:T(4,128)(2,1)} convert(f32[4,4,8]{2,1,0:T(4,128)} %get-tuple-element.9) | non-fusion elementwise | flops 128 | bytes 768 | tf_op jit(solution)/shard_map/convert_element_type | solution.py:454
  51.7 1.2 %copy.20 = f32[4,4]{1,0:T(4,128)} copy(f32[4,4]{1,0:T(4,128)} %get-tuple-element.18) | data formatting | bytes 128
  53.0 1.2 %copy.21 = bf16[4,128]{1,0:T(4,128)(2,1)} copy(bf16[4,128]{1,0:T(4,128)(2,1)} %get-tuple-element.19) | data formatting | bytes 2048

commit v3 on v2

--- a/solution.py
+++ b/solution.py
@@ -9,6 +9,7 @@
 
 EDGE = 16
 NOTE_ROWS = 4
+SMALL = 10
 
 
 def log_sigmoid(x):
@@ -29,6 +30,22 @@
     key_weight,
     value_weight,
     out_weight,
+    *rest,
+):
+    operands, rest = rest[:SMALL], rest[SMALL:]
+    outs, rest = rest[:4], rest[4:]
+    held, rest = rest[:SMALL], rest[SMALL:]
+    work(sp_count, tp_count, prompt, key_weight, value_weight, out_weight, operands, *held, *outs, *rest)
+
+
+def work(
+    sp_count,
+    tp_count,
+    prompt,
+    key_weight,
+    value_weight,
+    out_weight,
+    operands,
     input_weight,
     forget_weight,
     bias,
@@ -61,6 +78,7 @@
     halo_in,
     parts_out,
     parts_in,
+    small_sem,
     row_sem,
     edge_sem,
     weight_sem,
@@ -106,19 +124,36 @@
         for s in range(seqs)
         for side, start in enumerate((0, seg - EDGE))
     ]
-    key_copy.start()
+    smalls = (
+        input_weight,
+        forget_weight,
+        bias,
+        taps,
+        extra,
+        new_query,
+        new_key,
+        new_value,
+        new_input,
+        new_forget,
+    )
+    small_copies = [
+        pltpu.make_async_copy(source, here, small_sem.at[i])
+        for i, (source, here) in enumerate(zip(operands, smalls))
+    ]
+    for copy in small_copies:
+        copy.start()
     for copy in edge_copies:
         copy.start()
+    key_copy.start()
     pltpu.make_async_copy(prompt.at[0], rows.at[0], row_sem.at[0]).start()
     value_copy.start()
-    for s in range(1, seqs):
-        pltpu.make_async_copy(prompt.at[s], rows.at[s], row_sem.at[s]).start()
-    out_copy.start()
     lax.fori_loop(1, total, greet, 0)
 
     place = lax.broadcasted_iota(jnp.int32, (seg, seg), 0)
     other = lax.broadcasted_iota(jnp.int32, (seg, seg), 1)
     later[...] = jnp.where(place > other, 1.0, 0.0).astype(bf16)
+    for copy in small_copies:
+        copy.wait()
     gate_rows = jnp.concatenate(
         [forget_weight[...].astype(f32), input_weight[...].astype(f32)], axis=0
     )
@@ -209,6 +244,15 @@
 
     def sequence(s, carry):
         pltpu.make_async_copy(prompt.at[s], rows.at[s], row_sem.at[s]).wait()
+
+        @pl.when(s + 1 < seqs)
+        def _():
+            pltpu.make_async_copy(prompt.at[s + 1], rows.at[s + 1], row_sem.at[s + 1]).start()
+
+        @pl.when(s + 1 == seqs)
+        def _():
+            out_copy.start()
+
         lax.fori_loop(0, seg // block, project, s)
 
         @pl.when(s == 0)
@@ -266,14 +310,6 @@
         return lax.fori_loop(1, sp_count, send, carry)
 
     lax.fori_loop(0, seqs, sequence, 0)
-    out_copy.wait()
-
-    def arrive(i, c):
-        s = i // (sp_count - 1)
-        q = lax.rem(sp + 1 + lax.rem(i, sp_count - 1), sp_count)
-        note_copy(s, q, q).wait()
-        share_copy(s, q, q).wait()
-        return c
 
     queries, keys = (
         jnp.concatenate([ref[:, h, :].astype(f32) for h in range(heads)], axis=1)
@@ -288,12 +324,15 @@
             out = jnp.where(lane_head == h, column(new_value[s, h : h + 1, :].astype(f32)), out)
         fresh.append(out)
 
-    lax.fori_loop(0, seqs * (sp_count - 1), arrive, 0)
 
     depth = heads * cols
     lane = lax.broadcasted_iota(jnp.int32, (depth, 128), 1)
     reads = jnp.zeros((depth, 128), f32)
     for s in range(seqs):
+        for o in range(1, sp_count):
+            q = lax.rem(sp + o, sp_count)
+            note_copy(s, q, q).wait_recv()
+            share_copy(s, q, q).wait_recv()
         tail = jnp.zeros((1, lanes), f32)
         tops = [None] * sp_count
         for d in reversed(range(sp_count)):
@@ -330,6 +369,7 @@
         reads = jnp.where(lane == s, jnp.concatenate(found, axis=0), reads)
     if depth < 128:
         reads = jnp.concatenate([reads, jnp.zeros((128 - depth, 128), f32)], axis=0)
+    out_copy.wait()
     left = reads.T[:8, :depth].astype(bf16)
     partial = jnp.dot(left, wo[...], preferred_element_type=f32)
     features = read_out.shape[1]
@@ -347,18 +387,24 @@
             device_id_type=pl.DeviceIdType.MESH,
         )
 
-    def send_part(o, c):
-        part_copy(lax.rem(me + o, total), me).start()
-        return c
-
-    def take_part(o, c):
-        j = lax.rem(me + o, total)
-        part_copy(j, j).wait()
-        return c
-
-    lax.fori_loop(1, total, send_part, 0)
-    lax.fori_loop(1, total, take_part, 0)
+    others = [lax.rem(me + o, total) for o in range(1, total)]
+    for j in others:
+        part_copy(j, me).start()
+    for s in range(seqs):
+        for o in range(1, sp_count):
+            q = lax.rem(sp + o, sp_count)
+            note_copy(s, q, q).wait_send()
+            share_copy(s, q, q).wait_send()
+    for j in others:
+        part_copy(j, j).wait_send()
+    for j in others:
+        part_copy(j, j).wait_recv()
     read_out[...] = jnp.sum(parts_in[...], axis=0).astype(bf16)
+
+
+def finish(*refs):
+    for source, out in zip(refs[:4], refs[4:]):
+        out[...] = source[...].astype(out.dtype)
 
 
 def body(
@@ -389,6 +435,18 @@
     out_width = out_weight.shape[2]
     features = out_width // total
 
+    smalls = (
+        input_gate_weight.T,
+        forget_gate_weight.T,
+        forget_bias.reshape(1, heads),
+        key_taps,
+        extra_decay.transpose(0, 2, 1),
+        new_query,
+        new_key,
+        new_value,
+        new_input_gate,
+        new_forget_gate,
+    )
     vmem = pl.BlockSpec(memory_space=pltpu.VMEM)
     hbm = pl.BlockSpec(memory_space=pl.ANY)
     memory, normer, peak, read = pl.pallas_call(
@@ -399,9 +457,10 @@
             jax.ShapeDtypeStruct((seqs, heads), f32),
             jax.ShapeDtypeStruct((seqs, features), bf16),
         ),
-        in_specs=[hbm] * 4 + [vmem] * 10,
+        in_specs=[hbm] * (4 + SMALL),
         out_specs=[vmem] * 4,
-        scratch_shapes=[
+        scratch_shapes=[pltpu.VMEM(x.shape, x.dtype) for x in smalls]
+        + [
             pltpu.VMEM((seqs, seg, width), bf16),
             pltpu.VMEM((2 * seqs, EDGE, width), bf16),
             pltpu.VMEM((width, lanes), bf16),
@@ -420,6 +479,7 @@
             pltpu.VMEM((2, seqs, lanes), f32),
             pltpu.VMEM((total, seqs, features), f32),
             pltpu.VMEM((total, seqs, features), f32),
+            pltpu.SemaphoreType.DMA((SMALL,)),
             pltpu.SemaphoreType.DMA((seqs,)),
             pltpu.SemaphoreType.DMA((2 * seqs,)),
             pltpu.SemaphoreType.DMA((3,)),
@@ -440,18 +500,20 @@
         key_weight,
         value_weight,
         out_weight.reshape(depth, out_width),
-        input_gate_weight.T,
-        forget_gate_weight.T,
-        forget_bias.reshape(1, heads),
-        key_taps,
-        extra_decay.transpose(0, 2, 1),
-        new_query,
-        new_key,
-        new_value,
-        new_input_gate,
-        new_forget_gate,
-    )
-    return (memory.transpose(0, 1, 3, 2).astype(bf16), normer.astype(bf16), peak, read)
+        *smalls,
+    )
+    memory, normer, peak, read = pl.pallas_call(
+        finish,
+        out_shape=(
+            jax.ShapeDtypeStruct(memory.shape, bf16),
+            jax.ShapeDtypeStruct(normer.shape, bf16),
+            jax.ShapeDtypeStruct(peak.shape, f32),
+            jax.ShapeDtypeStruct(read.shape, bf16),
+        ),
+        in_specs=[vmem] * 4,
+        out_specs=[vmem] * 4,
+    )(memory, normer, peak, read)
+    return memory.transpose(0, 1, 3, 2), normer, peak, read
 
 
 def solution(mesh):

time: 54.5 us -> 46.6 us (0.86)
  other arithmetic: 2.84 us -> 0 us
  Pallas kernels: 48.3 us -> 45.8 us
  local copies, waits for them, and re-layouts: 2.43 us -> 0 us
    pallas_call x1, Pallas kernels: 48.3 us -> 44.2 us  [body(): pl.pallas_call(functools.partial(kernel, sp_count, tp_count), out_shape=(...]
    convert_element_type x2 -> x0, other arithmetic: 2.84 us -> none  [the longest x1 1.54 us: body(): memory.transpose(0, 1, 3, 2).astype(bf16)]
    unnamed x2 -> x0, local copies, waits for them, and re-layouts: 2.43 us -> none
    pallas_call x0 -> x1, Pallas kernels: none -> 1.58 us  [body(): pl.pallas_call(finish, out_shape=(jax.ShapeDtypeStruct(memory.shape, bf16...]
where the time goes in v3:
time: 46.6 us; the launch traced here: 46.4 us
  Pallas kernels  45.8 us (98%)
  between operations  0.64 us (1%)
    pallas_call x1, Pallas kernels, body(): pl.pallas_call(functools.partial(kernel, sp_count, tp_count), out_shape=(...  44.2 us
    pallas_call x1, Pallas kernels, body(): pl.pallas_call(finish, out_shape=(jax.ShapeDtypeStruct(memory.shape, bf16...  1.58 us

profile of v3, /device:TPU:0, one launch (start us, length us, event | category | flops | bytes accessed | tf_op | source)
XLA Modules:
  0.0 46.4 jit_solution(15333914918219378707)
XLA Ops:
  0.6 44.2 %shard_map.165 = (f32[4,4,16,64]{3,2,1,0:T(8,128)}, f32[4,4,8]{2,1,0:T(4,128)}, f32[4,4]{1,0:T(4,128)}, bf16[4,128]{1,0:T(4,128)(2,1)}) custom-call(bf16[4,512,4096]{2,1,0:T(8,128)(2,1)} %prompt.1, bf16[4096,256]{1,0:T(8,128)(2,1)} %key_weight.1, bf16[4096,512]{1,0:T(8,128)(2,1)} %value_weight.1, bf16[64,4096]{1,0:T(8,128)(2,1)} %bitcast.6, ...), custom_call_target="tpu_custom_call" | custom-call | tf_op jit(solution)/shard_map/pallas_call | solution.py:452
  44.9 1.6 %shard_map.166 = (bf16[4,4,16,64]{3,2,1,0:T(8,128)(2,1)}, bf16[4,4,8]{2,1,0:T(4,128)(2,1)}, f32[4,4]{1,0:T(4,128)}, bf16[4,128]{1,0:T(4,128)(2,1)}) custom-call(f32[4,4,16,64]{3,2,1,0:T(8,128)} %get-tuple-element.12.refs_0_, f32[4,4,8]{2,1,0:T(4,128)} %get-tuple-element.13.refs_1_, f32[4,4]{1,0:T(4,128)} %get-tuple-element.14.refs_2_, ...), custom_call_target="tpu_custom_call" | custom-call | tf_op jit(solution)/shard_map/pallas_call | solution.py:505
